TPU v7x, 32 devices: a whole 2x2x4 slice. The times are simulated.
32 devices in a mesh: sp: 8 (over z, y), tp: 4 (over x, core).
Axes of the slice: x: 2, y: 2, z: 4, core: 2. Of those that a mesh axis runs over, the one named last changes fastest.
Arguments:
- activations: bfloat16 [6144, 2048], P(('sp', 'tp')), may hold values from -6 to 6
- in_gain: float32 [2048], replicated, may hold values from 0.1 to 1.9
- w_pool_in: bfloat16 [2048, 1024], P(None, 'tp'), may hold values from -0.125 to 0.125
- pool_gain: float32 [1024], P('tp'), may hold values from 0.1 to 1.9
- w_qlat: bfloat16 [2048, 768], P(None, 'tp'), may hold values from -0.125 to 0.125
- w_kvlat: bfloat16 [2048, 512], P(None, 'tp'), may hold values from -0.125 to 0.125
- w_krope: bfloat16 [2048, 32], replicated, may hold values from -0.125 to 0.125
- qlat_gain: float32 [768], replicated, may hold values from 0.1 to 1.9
- kvlat_gain: float32 [512], replicated, may hold values from 0.1 to 1.9
- w_qup: bfloat16 [768, 1536], P(None, 'tp'), may hold values from -0.21875 to 0.21875
- w_kup: bfloat16 [512, 1024], P(None, 'tp'), may hold values from -0.25 to 0.25
- w_vup: bfloat16 [512, 1024], P(None, 'tp'), may hold values from -0.25 to 0.25
- qhead_gain: float32 [96], replicated, may hold values from 1.1 to 1.9
- khead_gain: float32 [96], replicated, may hold values from 1.1 to 1.9
- w_out_pool: bfloat16 [1024, 2048], P('tp'), may hold values from -0.1875 to 0.1875
- w_out_attn: bfloat16 [1024, 2048], P('tp'), may hold values from -0.75 to 0.75
Outputs:
- mixed: bfloat16 [6144, 2048], P(('sp', 'tp'))
All inputs are finite; a program needn't handle non-finite values.
Results may differ from a plain program's by a relative error of at most 0.025.
Values may be sent and summed in bfloat16 or wider, within the bound.
A program may use at most 128 MiB of HBM per device.

v0:
```python
import math
import jax
import jax.numpy as jnp
from jax import lax
from jax.sharding import PartitionSpec as P

GROUP = 256
NOPE = 64
ROPE = 32
VDIM = 64
QLAT = 768
KVLAT = 512
norm_eps = 1e-06
rope_theta = 10000.0
rim_depth = 15
block_rows = 512


def from_behind(block, axis, distance):
    devices = range(lax.axis_size(axis))
    route = [(i - distance, i) for i in devices if i - distance in devices]
    return lax.ppermute(block, axis, route)


def row_norm(source, norm_gain):
    as_float = source.astype(jnp.float32)
    factor = lax.rsqrt(jnp.mean(as_float * as_float, axis=-1, keepdims=True) + norm_eps)
    return as_float * factor * norm_gain


def rotate(head_rows, positions):
    half_rope = ROPE // 2
    frequency = rope_theta ** (-jnp.arange(0, ROPE, 2, dtype=jnp.float32) / ROPE)
    angles = positions.astype(jnp.float32)[:, None] * frequency[None, :]
    cosine = jnp.cos(angles)[:, None, :]
    sine_part = jnp.sin(angles)[:, None, :]
    plain_part = head_rows[..., :NOPE]
    lower_half = head_rows[..., NOPE : NOPE + half_rope]
    upper_half = head_rows[..., NOPE + half_rope :]
    return jnp.concatenate(
        [
            plain_part,
            lower_half * cosine - upper_half * sine_part,
            upper_half * cosine + lower_half * sine_part,
        ],
        axis=-1,
    )


def pool_mix(extended, positions, channel_start):
    row_count = positions.shape[0]
    width = extended.shape[1]
    channel = channel_start + jnp.arange(width, dtype=jnp.int32)
    window = jnp.left_shift(jnp.int32(2), channel // GROUP)
    as_float = extended.astype(jnp.float32)
    window_sum = jnp.zeros((row_count, width), jnp.float32)
    for lag_index in range(rim_depth + 1):
        lagged = as_float[rim_depth - lag_index : rim_depth - lag_index + row_count]
        window_sum = window_sum + jnp.where(lag_index < window[None, :], lagged, 0.0)
    divisor = jnp.minimum(positions[:, None] + 1, window[None, :]).astype(jnp.float32)
    return window_sum / divisor - as_float[rim_depth:]


def make_queries(q_normed, w_qup, norm_gain, positions):
    row_count = q_normed.shape[0]
    head_count = w_qup.shape[1] // (NOPE + ROPE)
    query_raw = jnp.dot(q_normed, w_qup, preferred_element_type=jnp.float32).astype(jnp.bfloat16)
    query_raw = query_raw.reshape(row_count, head_count, NOPE + ROPE)
    return rotate(row_norm(query_raw, norm_gain), positions).astype(jnp.bfloat16)


def plain_parts(kv_rows, w_kup, w_vup):
    key_plain = jnp.dot(kv_rows, w_kup, preferred_element_type=jnp.float32).astype(jnp.bfloat16)
    value_rows = jnp.dot(kv_rows, w_vup, preferred_element_type=jnp.float32).astype(jnp.bfloat16)
    return (key_plain, value_rows)


def finish_keys(key_plain, rope_rows, norm_gain, positions):
    row_count = key_plain.shape[0]
    head_count = key_plain.shape[1] // NOPE
    key_plain = key_plain.reshape(row_count, head_count, NOPE)
    shared = jnp.broadcast_to(rope_rows[:, None, :], (row_count, head_count, ROPE))
    joined = jnp.concatenate([key_plain, shared], axis=-1)
    key_rows = rotate(row_norm(joined, norm_gain), positions).astype(jnp.bfloat16)
    return key_rows.reshape(row_count, head_count * (NOPE + ROPE))


def update(state_pair, queries, query_pos, key_rows, value_rows, key_pos):
    numerator, denominator = state_pair
    head_count = queries.shape[1]
    key_rows = key_rows.reshape(key_rows.shape[0], head_count, NOPE + ROPE)
    value_rows = value_rows.reshape(value_rows.shape[0], head_count, VDIM)
    scores = jnp.einsum("qhd,khd->hqk", queries, key_rows, preferred_element_type=jnp.float32)
    scores = scores * (NOPE + ROPE) ** (-0.5)
    weights = jnp.where(key_pos[None, None, :] <= query_pos[None, :, None], jnp.exp(scores), 0.0)
    denominator = denominator + jnp.sum(weights, axis=-1)
    numerator = numerator + jnp.einsum(
        "hqk,khd->qhd", weights.astype(jnp.bfloat16), value_rows, preferred_element_type=jnp.float32
    )
    return (numerator, denominator)


def sweep(state_pair, pieces, expand, queries, query_pos):
    shard_rows = queries.shape[0]
    piece_rows = pieces[0].shape[0]
    block_size = shard_rows * math.gcd(piece_rows // shard_rows, max(1, block_rows // shard_rows))

    def advance(block_index, current):
        offset = block_index * block_size

        def accumulate(inner):
            chosen = tuple(
                (lax.dynamic_slice_in_dim(member, offset, block_size, 0) for member in pieces)
            )
            key_pos = offset + jnp.arange(block_size, dtype=jnp.int32)
            key_rows, value_rows = expand(chosen, key_pos)
            return update(inner, queries, query_pos, key_rows, value_rows, key_pos)

        def unchanged(inner):
            return inner

        return lax.cond(offset <= query_pos[-1], accumulate, unchanged, current)

    return lax.fori_loop(0, piece_rows // block_size, advance, state_pair)


def local(
    activations,
    in_gain,
    w_pool_in,
    pool_gain,
    w_qlat,
    w_kvlat,
    w_krope,
    qlat_gain,
    kvlat_gain,
    w_qup,
    w_kup,
    w_vup,
    qhead_gain,
    khead_gain,
    w_out_pool,
    w_out_attn,
):
    own_input = lax.all_gather(activations, "tp", axis=0, tiled=True)
    row_count = own_input.shape[0]
    positions = lax.axis_index("sp") * row_count + jnp.arange(row_count, dtype=jnp.int32)
    normed = row_norm(own_input, in_gain).astype(jnp.bfloat16)
    pool_in = jnp.dot(normed, w_pool_in, preferred_element_type=jnp.float32).astype(jnp.bfloat16)
    prev_rows = from_behind(pool_in[row_count - rim_depth :], "sp", 1)
    extended = jnp.concatenate([prev_rows, pool_in], axis=0)
    channel_start = lax.axis_index("tp") * pool_in.shape[1]
    pool_out = (pool_mix(extended, positions, channel_start) * pool_gain).astype(jnp.bfloat16)
    q_part = jnp.dot(normed, w_qlat, preferred_element_type=jnp.float32).astype(jnp.bfloat16)
    kv_part = jnp.dot(normed, w_kvlat, preferred_element_type=jnp.float32).astype(jnp.bfloat16)
    rope_key = jnp.dot(normed, w_krope, preferred_element_type=jnp.float32).astype(jnp.bfloat16)
    tp_index = lax.axis_index("tp")
    q_width = q_part.shape[1]
    kv_width = kv_part.shape[1]
    q_float = q_part.astype(jnp.float32)
    kv_float = kv_part.astype(jnp.float32)
    q_squares, kv_squares = lax.psum(
        (jnp.sum(q_float * q_float, axis=1), jnp.sum(kv_float * kv_float, axis=1)), "tp"
    )
    q_gain = lax.dynamic_slice_in_dim(qlat_gain, tp_index * q_width, q_width)
    kv_gain = lax.dynamic_slice_in_dim(kvlat_gain, tp_index * kv_width, kv_width)
    q_scaled = q_float * lax.rsqrt(q_squares / QLAT + norm_eps)[:, None] * q_gain
    kv_scaled = kv_float * lax.rsqrt(kv_squares / KVLAT + norm_eps)[:, None] * kv_gain
    q_normed, kv_normed = (
        lax.all_gather(q_scaled.astype(jnp.bfloat16), "tp", axis=1, tiled=True),
        lax.all_gather(kv_scaled.astype(jnp.bfloat16), "tp", axis=1, tiled=True),
    )
    queries = make_queries(q_normed, w_qup, qhead_gain, positions)
    head_count = queries.shape[1]
    start_pair = (
        jnp.zeros((row_count, head_count, VDIM), jnp.float32),
        jnp.zeros((head_count, row_count), jnp.float32),
    )
    key_plain, value_rows = plain_parts(kv_normed, w_kup, w_vup)

    def expand_plain(chosen, key_pos):
        return (finish_keys(chosen[0], chosen[2], khead_gain, key_pos), chosen[1])

    numerator, denominator = sweep(
        start_pair,
        (
            lax.all_gather(key_plain, "sp", axis=0, tiled=True),
            lax.all_gather(value_rows, "sp", axis=0, tiled=True),
            lax.all_gather(rope_key, "sp", axis=0, tiled=True),
        ),
        expand_plain,
        queries,
        positions,
    )
    attended = (numerator / jnp.transpose(denominator)[:, :, None]).astype(jnp.bfloat16)
    attended = attended.reshape(row_count, head_count * VDIM)
    term = jnp.dot(pool_out, w_out_pool, preferred_element_type=jnp.float32)
    return lax.psum_scatter(
        (term + jnp.dot(attended, w_out_attn, preferred_element_type=jnp.float32)).astype(
            jnp.bfloat16
        ),
        "tp",
        scatter_dimension=0,
        tiled=True,
    )


def solution(mesh):
    placed = (
        P(("sp", "tp"), None),
        P(),
        P(None, "tp"),
        P("tp"),
        P(None, "tp"),
        P(None, "tp"),
        P(),
        P(),
        P(),
        P(None, "tp"),
        P(None, "tp"),
        P(None, "tp"),
        P(),
        P(),
        P("tp", None),
        P("tp", None),
    )
    return jax.shard_map(
        local, mesh=mesh, in_specs=placed, out_specs=P(("sp", "tp"), None), check_vma=False
    )
```

profile of v0, /device:TPU:0, one launch (start us, length us, event | category | flops | bytes accessed | tf_op | source)
XLA Modules:
  0.0 318.9 jit_solution(7002376077708482121)
XLA Ops:
  6.5 0.7 all-gather.5.cloned.1.call-update
  7.3 0.8 dynamic_slice.16
  8.1 32.1 %all-gather.5.cloned.1.call-done = bf16[768,2048]{1,0:T(8,128)(2,1)} async-done(((bf16[192,2048]{1,0:T(8,128)(2,1)}), bf16[768,2048]{1,0:T(8,128)(2,1)}) %all-gather.5.cloned.1.call-update) | async-done | bytes 3145744 | tf_op jit(solution)/shard_map/all_gather | solution.py:145
  40.2 2.7 fusion.23
  43.0 0.8 fusion.25
  44.0 1.2 multiply_reduce_fusion.1
  45.7 1.2 multiply_reduce_fusion
  46.9 6.0 %all-reduce = (f32[768]{0:T(1024)S(1)}, f32[768]{0:T(1024)S(1)}) all-reduce(f32[768]{0:T(1024)S(1)} %get-tuple-element.242, f32[768]{0:T(1024)S(1)} %get-tuple-element.244), channel_id=1, replica_groups=mesh['sp'=8,'tp'=4] {'tp'}, use_global_device_ids=true, to_apply=%region_2.3 | all-reduce | flops 1536 | bytes 12288 | tf_op jit(solution)/shard_map/psum | solution.py:162
  53.0 0.8 multiply_convert_fusion
  53.9 0.8 dynamic_slice.15
  54.8 8.7 %all_gather.19 = bf16[768,512]{0,1:T(8,128)(2,1)S(1)} all-gather(bf16[768,128]{0,1:T(8,128)(2,1)S(1)} %multiply_convert_fusion.1), channel_id=1, replica_groups=mesh['sp'=8,'tp'=4] {'tp'}, dimensions={1}, use_global_device_ids=true | all-gather | bytes 983040 | tf_op jit(solution)/shard_map/all_gather | solution.py:171
  63.5 1.2 convolution_convert_fusion.2
  64.8 2.1 convolution_convert_fusion.1
  67.5 3.1 convolution_convert_fusion.3
  70.6 3.4 %collective-permute-start = (bf16[15,256]{1,0:T(8,128)(2,1)S(1)}, bf16[15,256]{1,0:T(8,128)(2,1)S(1)}, u32[]{:S(2)}, u32[]{:S(2)}) collective-permute-start(bf16[15,256]{1,0:T(8,128)(2,1)S(1)} %slice.102), channel_id=1, source_target_pairs={{0,4},{4,8},{8,12},{12,16},{16,20},{20,24},{24,28},{1,5},{5,9},{9,... | collective-permute-start | bytes 23048 | tf_op jit(solution)/shard_map/ppermute | solution.py:22
  74.0 1.0 convolution_convert_fusion.6
  75.1 32.1 %all_gather.22 = bf16[6144,32]{0,1:T(8,128)(2,1)S(1)} all-gather(bf16[768,32]{0,1:T(8,128)(2,1)S(1)} %convolution_convert_fusion.6), channel_id=1, replica_groups=mesh['sp'=8,'tp'=4] {'sp'}, dimensions={0}, use_global_device_ids=true | all-gather | bytes 442368 | tf_op jit(solution)/shard_map/all_gather | solution.py:189
  107.3 5.2 %fusion.49 = f32[768,2048]{1,0:T(8,128)} fusion(bf16[256,2048]{1,0:T(8,128)(2,1)S(1)} %copy-done, f32[783,256]{1,0:T(8,128)S(1)} %maximum_convert_fusion, f32[256]{0:T(256)S(1)} %copy-done.15, s32[256]{0:T(256)S(1)} %fusion.69, s32[768]{0:T(1024)S(1)} %fusion.68, pred[256]{0:T(512)(128)(4,1)S(1)} %get-tuple-element.246, ...), kind=kOutput, calls=%fused_computation.95 | convolution fusion | flops 812580864 | bytes 19937280 | tf_op jit(solution)/shard_map/dot_general | solution.py:197
  112.6 2.0 convolution_convert_fusion
  115.0 0.9 pad_maximum_fusion.1
  115.8 20.9 %all-gather.7.cloned.1.call-done = bf16[6144,256]{1,0:T(8,128)(2,1)} async-done(((bf16[768,256]{1,0:T(8,128)(2,1)}), bf16[6144,256]{1,0:T(8,128)(2,1)}) %all-gather.7.cloned.1.call-update) | async-done | bytes 3145744 | tf_op jit(solution)/shard_map/all_gather | solution.py:188
  136.7 4.6 %copy.18 = bf16[6144,256]{0,1:T(8,128)(2,1)} copy(bf16[6144,256]{1,0:T(8,128)(2,1)} %all-gather.7.cloned.1.call-done) | data formatting | bytes 6291456 | tf_op jit(solution)/shard_map/while | solution.py:124
  141.3 56.1 %all-gather.9.cloned.1.call-done = bf16[6144,256]{1,0:T(8,128)(2,1)} async-done(((bf16[768,256]{1,0:T(8,128)(2,1)}), bf16[6144,256]{1,0:T(8,128)(2,1)}) %all-gather.9.cloned.1.call-update) | async-done | bytes 3145744 | tf_op jit(solution)/shard_map/all_gather | solution.py:187
  197.5 4.7 %copy.19 = bf16[6144,256]{0,1:T(8,128)(2,1)} copy(bf16[6144,256]{1,0:T(8,128)(2,1)} %all-gather.9.cloned.1.call-done) | data formatting | bytes 6291456 | tf_op jit(solution)/shard_map/while | solution.py:124
  202.2 17.4 %while.15 = (s32[]{:T(128)}, f32[768,4,64]{0,2,1:T(8,128)S(1)}, f32[4,768]{1,0:T(4,128)S(1)}, s32[768]{0:T(1024)S(1)}, bf16[6144,256]{0,1:T(8,128)(2,1)}, /*inde...) while((s32[]{:T(128)}, f32[768,4,64]{0,2,1:T(8,128)S(1)}, ...), condition=%wide.region_11.12_spmd, body=%wide.region_6.11_spmd.sunk | while | flops 775635520 | bytes 32112456 | solution.py:124
  203.5 7.2 %conditional.2 = ((f32[768,4,64]{0,2,1:T(8,128)S(1)}, f32[4,768]{1,0:T(4,128)S(1)})) conditional(s32[]{:T(128)} %convert_element_type.159, (f32[768,4,64]{0,2,1:T(8,128)S(1)}, f32[4,768]{1,0:T(4,128)S(1)}) %tuple.55, (s32[]{:T(128)}, bf16[6144,256]{0,1:T(8,128)(2,1)}, s32[768]{0:T(1024)S(1)}, bf16[6144,256]{0,1:T(8,128)(2,1)}, ...), branch_computations={%region_7.7_spmd, %region_8.10_spmd} | conditional | flops 775635520 | bytes 32112226 | solution.py:122
  203.6 1.2 constant_dynamic-slice_fusion.1
  205.9 2.6 fusion
  208.6 2.1 fusion.8
  212.0 0.6 slice.263
  219.7 5.5 %add_convert_fusion.1 = bf16[768,2048]{1,0:T(8,128)(2,1)} fusion(f32[768,2048]{1,0:T(8,128)} %fusion.49, bf16[768,256]{0,1:T(8,128)(2,1)S(1)} %bitcast.48, bf16[256,2048]{1,0:T(8,128)(2,1)S(1)} %copy-done.4), kind=kOutput, calls=%fused_computation.39 | convolution fusion | flops 808452096 | bytes 10878976 | tf_op jit(solution)/shard_map/dot_general | solution.py:199
  225.2 87.2 %reduce-scatter.2.cloned.1.call-done = bf16[192,2048]{1,0:T(8,128)(2,1)} async-done(((bf16[768,2048]{1,0:T(8,128)(2,1)}), bf16[192,2048]{1,0:T(8,128)(2,1)}) %reduce-scatter.2.cloned.1.call-update) | async-done | bytes 786448 | tf_op jit(solution)/shard_map/reduce_scatter | solution.py:198
  (97 shorter events, 7.8 us)
Async XLA Ops:
  6.5 100.8 %copy-start = (bf16[256,2048]{1,0:T(8,128)(2,1)S(1)}, bf16[256,2048]{1,0:T(8,128)(2,1)}, u32[]{:S(2)}) copy-start(bf16[256,2048]{1,0:T(8,128)(2,1)} %param.34) | copy-start | bytes 3145732
  6.5 36.4 %copy-start.9 = (f32[2048]{0:T(1024)S(1)}, f32[2048]{0:T(1024)}, u32[]{:S(2)}) copy-start(f32[2048]{0:T(1024)} %param.21) | copy-start | bytes 24580
  6.5 33.6 %all-gather.5.cloned.1.call-start = ((), (), s32[]{:S(2)}) async-start(), calls=%async_computation.1 | async-start | bytes 3932160 | tf_op jit(solution)/shard_map/all_gather | solution.py:145
  7.3 105.3 %all-gather.11.cloned.1.call-start = ((), (), s32[]{:S(2)}) async-start(), calls=%async_computation.4 | async-start | bytes 1474560 | tf_op jit(solution)/shard_map/all_gather | solution.py:170
  40.2 2.8 copy-start.3
  43.0 1.0 copy-start.6
  44.0 2.9 copy-start.1
  44.0 1.7 copy-start.12
  45.7 17.8 %copy-start.14 = (bf16[512,256]{1,0:T(8,128)(2,1)S(1)}, bf16[512,256]{1,0:T(8,128)(2,1)}, u32[]{:S(2)}) copy-start(bf16[512,256]{1,0:T(8,128)(2,1)} %param.31) | copy-start | bytes 786436
  53.8 13.7 %copy-start.11 = (bf16[2048,256]{1,0:T(8,128)(2,1)S(1)}, bf16[2048,256]{1,0:T(8,128)(2,1)}, u32[]{:S(2)}) copy-start(bf16[2048,256]{1,0:T(8,128)(2,1)} %param.22) | copy-start | bytes 3145732
  53.8 82.9 %all-gather.7.cloned.1.call-start = ((), (), s32[]{:S(2)}) async-start(), calls=%async_computation.2 | async-start | bytes 3538944 | tf_op jit(solution)/shard_map/all_gather | solution.py:188
  64.7 132.7 %all-gather.9.cloned.1.call-start = ((), (), s32[]{:S(2)}) async-start(), calls=%async_computation.3 | async-start | bytes 3538944 | tf_op jit(solution)/shard_map/all_gather | solution.py:187
  66.9 245.4 %reduce-scatter.2.cloned.1.call-start = ((), (), s32[]{:S(2)}) async-start(), calls=%async_computation.5 | async-start | bytes 3932160 | tf_op jit(solution)/shard_map/reduce_scatter | solution.py:198
  67.5 6.6 %copy-start.2 = (bf16[768,2048]{1,0:T(8,128)(2,1)S(1)}, bf16[768,2048]{1,0:T(8,128)(2,1)}, u32[]{:S(2)}) copy-start(bf16[768,2048]{1,0:T(8,128)(2,1)} %copy-done.1) | copy-start | bytes 9437188
  67.5 6.6 %copy-start.7 = (bf16[2048,32]{0,1:T(8,128)(2,1)S(1)}, bf16[2048,32]{0,1:T(8,128)(2,1)}, u32[]{:S(2)}) copy-start(bf16[2048,32]{0,1:T(8,128)(2,1)} %param.26) | copy-start | bytes 393220
  70.6 36.7 %copy-start.15 = (f32[256]{0:T(256)S(1)}, f32[256]{0:T(256)}, u32[]{:S(2)}) copy-start(f32[256]{0:T(256)} %param.23) | copy-start | bytes 3076
  70.6 36.6 %collective-permute-start = (bf16[15,256]{1,0:T(8,128)(2,1)S(1)}, bf16[15,256]{1,0:T(8,128)(2,1)S(1)}, u32[]{:S(2)}, u32[]{:S(2)}) collective-permute-start(bf16[15,256]{1,0:T(8,128)(2,1)S(1)} %slice.102), channel_id=1, source_target_pairs={{0,4},{4,8},{8,12},{12,16},{16,20},{20,24},{24,28},{1,5},{5,9},{9,... | collective-permute-start | bytes 23048 | tf_op jit(solution)/shard_map/ppermute | solution.py:22
  107.3 5.2 %copy-start.13 = (bf16[768,384]{1,0:T(8,128)(2,1)S(1)}, bf16[768,384]{1,0:T(8,128)(2,1)}, u32[]{:S(2)}) copy-start(bf16[768,384]{1,0:T(8,128)(2,1)} %param.29) | copy-start | bytes 1769476
  112.6 2.1 copy-start.10
  141.3 60.9 %copy-start.8 = (f32[96]{0:T(128)S(1)}, f32[96]{0:T(128)}, u32[]{:S(2)}) copy-start(f32[96]{0:T(128)} %param.33) | copy-start | bytes 1156
  202.2 17.4 %copy-start.4 = (bf16[256,2048]{1,0:T(8,128)(2,1)S(1)}, bf16[256,2048]{1,0:T(8,128)(2,1)}, u32[]{:S(2)}) copy-start(bf16[256,2048]{1,0:T(8,128)(2,1)} %param.35) | copy-start | bytes 3145732
  203.5 2.4 copy-start.5
Sparse Core Ops, SparseCore 0:
  8.9 31.2 all-gather.4
  53.9 18.5 all-gather.10
  74.7 61.9 all-gather.6
  138.7 58.6 all-gather.8
  225.3 86.9 reduce-scatter.1
where the time goes:
time: 320 us; the launch traced here: 319 us
  waiting for transfers between devices  197 us (62%)
  blocking collectives  46.9 us (15%)
  matrix products  27.2 us (8%)
  local copies, waits for them, and re-layouts  18.1 us (6%)
  between operations  13.5 us (4%)
  other arithmetic  7.26 us (2%)
  loops' own time  5.33 us (2%)
  starting transfers between devices  3.61 us (1%)
    reduce_scatter x1, waiting for transfers between devices, local(): lax.psum_scatter((term + jnp.dot(attended, w_out_attn, preferred_element_...  87.2 us
    all_gather x1, waiting for transfers between devices, local(): lax.all_gather(key_plain, 'sp', axis=0, tiled=True)  56.1 us
    all_gather x1, blocking collectives, local(): lax.all_gather(rope_key, 'sp', axis=0, tiled=True)  32.1 us
    all_gather x1, waiting for transfers between devices, local(): own_input = lax.all_gather(activations, 'tp', axis=0, tiled=True)  32.1 us
    all_gather x1, waiting for transfers between devices, local(): lax.all_gather(value_rows, 'sp', axis=0, tiled=True)  20.9 us
    while x2, local copies, waits for them, and re-layouts, sweep(): return lax.fori_loop(0, piece_rows // block_size, advance, state_pair)  9.32 us
    all_gather x1, blocking collectives, local(): lax.all_gather(kv_scaled.astype(jnp.bfloat16), 'tp', axis=1, tiled=True)  8.73 us
  transfers between devices with their start and end apart: 6, of which 4 were waited for; matrix products, arithmetic and copies ran while one was open for 7% of the time, Pallas kernels for 0%

commit v1 on v0

--- a/solution.py
+++ b/solution.py
@@ -142,7 +142,13 @@
     w_out_pool,
     w_out_attn,
 ):
-    own_input = lax.all_gather(activations, "tp", axis=0, tiled=True)
+    peers = lax.axis_size("tp")
+    held, blocks = (activations, [activations])
+    for _ in range(peers - 1):
+        held = lax.ppermute(held, "tp", [(i_2, (i_2 + 1) % peers) for i_2 in range(peers)])
+        blocks.insert(0, held)
+    line = jnp.concatenate(blocks, axis=0)
+    own_input = jnp.roll(line, (lax.axis_index("tp") + 1) * activations.shape[0], axis=0)
     row_count = own_input.shape[0]
     positions = lax.axis_index("sp") * row_count + jnp.arange(row_count, dtype=jnp.int32)
     normed = row_norm(own_input, in_gain).astype(jnp.bfloat16)

time: 320 us -> 324 us (1.012)
  local copies, waits for them, and re-layouts: 18.1 us -> 21.4 us
    ppermute x0 -> x3, waiting for transfers between devices: none -> 34 us  [local(): lax.ppermute(held, 'tp', [(i_2, (i_2 + 1) % peers) for i_2 in range(peers)])]
    all_gather x1 -> x0, waiting for transfers between devices: 32.1 us -> none  [local(): own_input = lax.all_gather(activations, 'tp', axis=0, tiled=True)]
  transfers between devices with their start and end apart: 6 -> 8, of which waited for: 4 -> 6; matrix products, arithmetic and copies ran while one was open for 7% -> 7% of each run, Pallas kernels for 0% -> 0%
where the time goes in v1:
time: 324 us
  waiting for transfers between devices  198 us (61%)
  blocking collectives  48.2 us (15%)
  matrix products  28.2 us (9%)
  local copies, waits for them, and re-layouts  21.4 us (7%)
  between operations  13.6 us (4%)
  loops' own time  5.42 us (2%)
  other arithmetic  5.02 us (2%)
  starting transfers between devices  4.2 us (1%)
    reduce_scatter x1, waiting for transfers between devices, local(): lax.psum_scatter((term + jnp.dot(attended, w_out_attn, preferred_element_...  87.1 us
    all_gather x1, waiting for transfers between devices, local(): lax.all_gather(key_plain, 'sp', axis=0, tiled=True)  56.2 us
    ppermute x3, waiting for transfers between devices, local(): lax.ppermute(held, 'tp', [(i_2, (i_2 + 1) % peers) for i_2 in range(peers)])  34 us
    all_gather x1, blocking collectives, local(): lax.all_gather(rope_key, 'sp', axis=0, tiled=True)  32.9 us
    all_gather x1, waiting for transfers between devices, local(): lax.all_gather(value_rows, 'sp', axis=0, tiled=True)  20.3 us
    all_gather x1, blocking collectives, local(): lax.all_gather(kv_scaled.astype(jnp.bfloat16), 'tp', axis=1, tiled=True)  9.41 us
    while x2, local copies, waits for them, and re-layouts, sweep(): return lax.fori_loop(0, piece_rows // block_size, advance, state_pair)  9.4 us
  transfers between devices with their start and end apart: 8, of which 6 were waited for; matrix products, arithmetic and copies ran while one was open for 7% of the time, Pallas kernels for 0%

profile of v1, /device:TPU:0, one launch (start us, length us, event | category | flops | bytes accessed | tf_op | source)
XLA Modules:
  0.0 323.7 jit_solution(10146911001589171603)
XLA Ops:
  7.0 11.8 %collective-permute-done = bf16[192,2048]{1,0:T(8,128)(2,1)S(1)} collective-permute-done((bf16[192,2048]{1,0:T(8,128)(2,1)}, bf16[192,2048]{1,0:T(8,128)(2,1)S(1)}, u32[]{:S(2)}, u32[]{:S(2)}) %collective-permute-start) | collective-permute-done | bytes 786464 | tf_op jit(solution)/shard_map/ppermute | solution.py:148
  18.9 11.4 %collective-permute-done.1 = bf16[192,2048]{1,0:T(8,128)(2,1)S(1)} collective-permute-done((bf16[192,2048]{1,0:T(8,128)(2,1)S(1)}, bf16[192,2048]{1,0:T(8,128)(2,1)S(1)}, u32[]{:S(2)}, u32[]{:S(2)}) %collective-permute-start.1) | collective-permute-done | bytes 786464 | tf_op jit(solution)/shard_map/ppermute | solution.py:148
  31.0 10.8 %collective-permute-done.2 = bf16[192,2048]{1,0:T(8,128)(2,1)} collective-permute-done((bf16[192,2048]{1,0:T(8,128)(2,1)S(1)}, bf16[192,2048]{1,0:T(8,128)(2,1)}, u32[]{:S(2)}, u32[]{:S(2)}) %collective-permute-start.2) | collective-permute-done | bytes 786464 | tf_op jit(solution)/shard_map/ppermute | solution.py:148
  41.8 1.2 constant_dynamic-update-slice_fusion.7
  43.2 1.2 constant_dynamic-update-slice_fusion.4
  44.4 1.2 constant_dynamic-update-slice_fusion.3
  45.8 1.3 fusion.23
  47.1 1.7 multiply_reduce_fusion.1
  48.9 1.7 multiply_reduce_fusion
  50.5 5.9 %all-reduce = (f32[768]{0:T(1024)S(1)}, f32[768]{0:T(1024)S(1)}) all-reduce(f32[768]{0:T(1024)S(1)} %get-tuple-element.242, f32[768]{0:T(1024)S(1)} %get-tuple-element.244), channel_id=1, replica_groups=mesh['sp'=8,'tp'=4] {'tp'}, use_global_device_ids=true, to_apply=%region_2.3 | all-reduce | flops 1536 | bytes 12288 | tf_op jit(solution)/shard_map/psum | solution.py:168
  56.5 0.8 multiply_convert_fusion
  58.2 9.4 %all_gather.15 = bf16[768,512]{0,1:T(8,128)(2,1)S(1)} all-gather(bf16[768,128]{0,1:T(8,128)(2,1)S(1)} %multiply_convert_fusion.1), channel_id=1, replica_groups=mesh['sp'=8,'tp'=4] {'tp'}, dimensions={1}, use_global_device_ids=true | all-gather | bytes 983040 | tf_op jit(solution)/shard_map/all_gather | solution.py:177
  67.6 1.2 convolution_convert_fusion.2
  68.9 1.2 convolution_convert_fusion.1
  70.6 3.7 %convolution_convert_fusion.3 = bf16[768,256]{1,0:T(8,128)(2,1)S(1)} fusion(bf16[2048,256]{1,0:T(8,128)(2,1)} %param.22, f32[2048]{0:T(1024)S(1)} %copy-done.13, f32[768]{0:T(1024)S(1)} %add_rsqrt_fusion.4, bf16[1536,2048]{1,0:T(8,128)(2,1)} %copy-done.2, s32[]{:T(128)S(6)} %select_n.136), kind=kOutput, calls=%fused_computation.45 | convolution fusion | flops 811794432 | bytes 4598788 | tf_op jit(solution)/shard_map/dot_general | solution.py:155
  74.4 3.6 %collective-permute-start.3 = (bf16[15,256]{1,0:T(8,128)(2,1)S(1)}, bf16[15,256]{1,0:T(8,128)(2,1)S(1)}, u32[]{:S(2)}, u32[]{:S(2)}) collective-permute-start(bf16[15,256]{1,0:T(8,128)(2,1)S(1)} %slice.102), channel_id=1, source_target_pairs={{0,4},{4,8},{8,12},{12,16},{16,20},{20,24},{24,28},{1,5},{5,9},{9,... | collective-permute-start | bytes 23048 | tf_op jit(solution)/shard_map/ppermute | solution.py:22
  78.0 1.4 convolution_convert_fusion.6
  79.4 32.9 %all_gather.18 = bf16[6144,32]{0,1:T(8,128)(2,1)S(1)} all-gather(bf16[768,32]{0,1:T(8,128)(2,1)S(1)} %convolution_convert_fusion.6), channel_id=1, replica_groups=mesh['sp'=8,'tp'=4] {'sp'}, dimensions={0}, use_global_device_ids=true | all-gather | bytes 442368 | tf_op jit(solution)/shard_map/all_gather | solution.py:195
  112.4 5.2 %fusion.49 = f32[768,2048]{1,0:T(8,128)} fusion(bf16[256,2048]{1,0:T(8,128)(2,1)S(1)} %copy-done, f32[783,256]{1,0:T(8,128)S(1)} %maximum_convert_fusion, f32[256]{0:T(256)S(1)} %copy-done.14, s32[256]{0:T(256)S(1)} %fusion.69, s32[768]{0:T(1024)S(1)} %fusion.68, pred[256]{0:T(512)(128)(4,1)S(1)} %get-tuple-element.246, ...), kind=kOutput, calls=%fused_computation.95 | convolution fusion | flops 812580864 | bytes 19937280 | tf_op jit(solution)/shard_map/dot_general | solution.py:203
  117.6 2.0 convolution_convert_fusion
  120.1 0.9 pad_maximum_fusion.1
  120.9 20.3 %all-gather.4.cloned.1.call-done = bf16[6144,256]{1,0:T(8,128)(2,1)} async-done(((bf16[768,256]{1,0:T(8,128)(2,1)}), bf16[6144,256]{1,0:T(8,128)(2,1)}) %all-gather.4.cloned.1.call-update) | async-done | bytes 3145744 | tf_op jit(solution)/shard_map/all_gather | solution.py:194
  141.2 4.7 %copy.18 = bf16[6144,256]{0,1:T(8,128)(2,1)} copy(bf16[6144,256]{1,0:T(8,128)(2,1)} %all-gather.4.cloned.1.call-done) | data formatting | bytes 6291456 | tf_op jit(solution)/shard_map/while | solution.py:124
  146.0 56.2 %all-gather.6.cloned.1.call-done = bf16[6144,256]{1,0:T(8,128)(2,1)} async-done(((bf16[768,256]{1,0:T(8,128)(2,1)}), bf16[6144,256]{1,0:T(8,128)(2,1)}) %all-gather.6.cloned.1.call-update) | async-done | bytes 3145744 | tf_op jit(solution)/shard_map/all_gather | solution.py:193
  202.1 4.6 %copy.19 = bf16[6144,256]{0,1:T(8,128)(2,1)} copy(bf16[6144,256]{1,0:T(8,128)(2,1)} %all-gather.6.cloned.1.call-done) | data formatting | bytes 6291456 | tf_op jit(solution)/shard_map/while | solution.py:124
  206.9 17.6 %while.15 = (s32[]{:T(128)}, f32[768,4,64]{0,2,1:T(8,128)S(1)}, f32[4,768]{1,0:T(4,128)S(1)}, s32[768]{0:T(1024)S(1)}, bf16[6144,256]{0,1:T(8,128)(2,1)}, /*inde...) while((s32[]{:T(128)}, f32[768,4,64]{0,2,1:T(8,128)S(1)}, ...), condition=%wide.region_11.12_spmd, body=%wide.region_6.11_spmd.sunk | while | flops 775635520 | bytes 32112456 | solution.py:124
  208.2 7.2 %conditional.2 = ((f32[768,4,64]{0,2,1:T(8,128)S(1)}, f32[4,768]{1,0:T(4,128)S(1)})) conditional(s32[]{:T(128)} %convert_element_type.175, (f32[768,4,64]{0,2,1:T(8,128)S(1)}, f32[4,768]{1,0:T(4,128)S(1)}) %tuple.55, (s32[]{:T(128)}, bf16[6144,256]{0,1:T(8,128)(2,1)}, s32[768]{0:T(1024)S(1)}, bf16[6144,256]{0,1:T(8,128)(2,1)}, ...), branch_computations={%region_7.7_spmd, %region_8.10_spmd} | conditional | flops 775635520 | bytes 32112226 | solution.py:122
  208.2 1.2 constant_dynamic-slice_fusion.1
  210.6 2.6 fusion
  213.3 2.1 fusion.8
  224.6 5.5 %add_convert_fusion.1 = bf16[768,2048]{1,0:T(8,128)(2,1)} fusion(f32[768,2048]{1,0:T(8,128)} %fusion.49, bf16[768,256]{0,1:T(8,128)(2,1)S(1)} %bitcast.46, bf16[256,2048]{1,0:T(8,128)(2,1)S(1)} %copy-done.3), kind=kOutput, calls=%fused_computation.39 | convolution fusion | flops 808452096 | bytes 10878976 | tf_op jit(solution)/shard_map/dot_general | solution.py:205
  230.1 87.1 %reduce-scatter.2.cloned.1.call-done = bf16[192,2048]{1,0:T(8,128)(2,1)} async-done(((bf16[768,2048]{1,0:T(8,128)(2,1)}), bf16[192,2048]{1,0:T(8,128)(2,1)}) %reduce-scatter.2.cloned.1.call-update) | async-done | bytes 786448 | tf_op jit(solution)/shard_map/reduce_scatter | solution.py:204
  (110 shorter events, 10.1 us)
Async XLA Ops:
  6.5 105.8 %copy-start = (bf16[256,2048]{1,0:T(8,128)(2,1)S(1)}, bf16[256,2048]{1,0:T(8,128)(2,1)}, u32[]{:S(2)}) copy-start(bf16[256,2048]{1,0:T(8,128)(2,1)} %param.34) | copy-start | bytes 3145732
  6.5 39.2 %copy-start.1 = (bf16[192,2048]{1,0:T(8,128)(2,1)S(1)}, bf16[192,2048]{1,0:T(8,128)(2,1)}, u32[]{:S(2)}) copy-start(bf16[192,2048]{1,0:T(8,128)(2,1)} %param.20) | copy-start | bytes 2359300
  6.5 111.1 %all-gather.8.cloned.1.call-start = ((), (), s32[]{:S(2)}) async-start(), calls=%async_computation.3 | async-start | bytes 1474560 | tf_op jit(solution)/shard_map/all_gather | solution.py:176
  6.5 12.3 %collective-permute-start = (bf16[192,2048]{1,0:T(8,128)(2,1)}, bf16[192,2048]{1,0:T(8,128)(2,1)S(1)}, u32[]{:S(2)}, u32[]{:S(2)}) collective-permute-start(bf16[192,2048]{1,0:T(8,128)(2,1)} %param.20), channel_id=1, source_target_pairs={{0,1},{1,2},{2,3},{3,0},{4,5},{5,6},{6,7},{7,4},{8,9},{9,10},{10,1... | collective-permute-start | bytes 2359304 | tf_op jit(solution)/shard_map/ppermute | solution.py:148
  18.9 11.4 %collective-permute-start.1 = (bf16[192,2048]{1,0:T(8,128)(2,1)S(1)}, bf16[192,2048]{1,0:T(8,128)(2,1)S(1)}, u32[]{:S(2)}, u32[]{:S(2)}) collective-permute-start(bf16[192,2048]{1,0:T(8,128)(2,1)S(1)} %collective-permute-done), channel_id=1, source_target_pairs={{0,1},{1,2},{2,3},{3,0},{4,5},{5,6},{6,7},{7,4},{8,9},{9,10},{10,1... | collective-permute-start | bytes 2359304 | tf_op jit(solution)/shard_map/ppermute | solution.py:148
  30.3 11.5 %collective-permute-start.2 = (bf16[192,2048]{1,0:T(8,128)(2,1)S(1)}, bf16[192,2048]{1,0:T(8,128)(2,1)}, u32[]{:S(2)}, u32[]{:S(2)}) collective-permute-start(bf16[192,2048]{1,0:T(8,128)(2,1)S(1)} %collective-permute-done.1), channel_id=1, source_target_pairs={{0,1},{1,2},{2,3},{3,0},{4,5},{5,6},{6,7},{7,4},{8,9},{9,10},{10,1... | collective-permute-start | bytes 2359304 | tf_op jit(solution)/shard_map/ppermute | solution.py:148
  43.1 4.1 %copy-start.9 = (bf16[2048,128]{1,0:T(8,128)(2,1)S(1)}, bf16[2048,128]{1,0:T(8,128)(2,1)}, u32[]{:S(2)}) copy-start(bf16[2048,128]{1,0:T(8,128)(2,1)} %param.25) | copy-start | bytes 1572868
  43.1 4.1 %copy-start.13 = (f32[2048]{0:T(1024)S(1)}, f32[2048]{0:T(1024)}, u32[]{:S(2)}) copy-start(f32[2048]{0:T(1024)} %param.21) | copy-start | bytes 24580
  45.7 3.2 copy-start.7
  45.8 4.7 %copy-start.2 = (bf16[1536,2048]{1,0:T(8,128)(2,1)}, bf16[1536,2048]{1,0:T(8,128)(2,1)S(1)}, u32[]{:S(2)}) copy-start(bf16[1536,2048]{1,0:T(8,128)(2,1)S(1)} %constant_dynamic-update-slice_fusion) | copy-start | bytes 18874372
  48.8 18.8 %copy-start.10 = (bf16[512,256]{1,0:T(8,128)(2,1)S(1)}, bf16[512,256]{1,0:T(8,128)(2,1)}, u32[]{:S(2)}) copy-start(bf16[512,256]{1,0:T(8,128)(2,1)} %param.31) | copy-start | bytes 786436
  48.8 20.1 %copy-start.11 = (bf16[512,256]{1,0:T(8,128)(2,1)S(1)}, bf16[512,256]{1,0:T(8,128)(2,1)}, u32[]{:S(2)}) copy-start(bf16[512,256]{1,0:T(8,128)(2,1)} %param.30) | copy-start | bytes 786436
  57.3 83.9 %all-gather.4.cloned.1.call-start = ((), (), s32[]{:S(2)}) async-start(), calls=%async_computation.1 | async-start | bytes 3538944 | tf_op jit(solution)/shard_map/all_gather | solution.py:194
  68.8 133.3 %all-gather.6.cloned.1.call-start = ((), (), s32[]{:S(2)}) async-start(), calls=%async_computation.2 | async-start | bytes 3538944 | tf_op jit(solution)/shard_map/all_gather | solution.py:193
  70.1 7.9 %slice-start = ((s8[6291456]{0:T(1024)(128)(4,1)}), s8[2097152]{0:T(1024)(128)(4,1)S(1)}, s32[]{:S(2)}) async-start(s8[6291456]{0:T(1024)(128)(4,1)} %bitcast.42), calls=%async_computation.5 | async-start | bytes 4194304
  70.1 7.9 %copy-start.12 = (bf16[2048,32]{0,1:T(8,128)(2,1)S(1)}, bf16[2048,32]{0,1:T(8,128)(2,1)}, u32[]{:S(2)}) copy-start(bf16[2048,32]{0,1:T(8,128)(2,1)} %param.26) | copy-start | bytes 393220
  70.1 247.1 %reduce-scatter.2.cloned.1.call-start = ((), (), s32[]{:S(2)}) async-start(), calls=%async_computation.4 | async-start | bytes 3932160 | tf_op jit(solution)/shard_map/reduce_scatter | solution.py:204
  70.6 7.3 %slice-start.1 = ((s8[6291456]{0:T(1024)(128)(4,1)}), s8[4194304]{0:T(1024)(128)(4,1)S(1)}, s32[]{:S(2)}) async-start(s8[6291456]{0:T(1024)(128)(4,1)} %bitcast.42), calls=%async_computation.6 | async-start | bytes 8388608
  74.3 38.0 %copy-start.14 = (f32[256]{0:T(256)S(1)}, f32[256]{0:T(256)}, u32[]{:S(2)}) copy-start(f32[256]{0:T(256)} %param.23) | copy-start | bytes 3076
  74.4 37.9 %collective-permute-start.3 = (bf16[15,256]{1,0:T(8,128)(2,1)S(1)}, bf16[15,256]{1,0:T(8,128)(2,1)S(1)}, u32[]{:S(2)}, u32[]{:S(2)}) collective-permute-start(bf16[15,256]{1,0:T(8,128)(2,1)S(1)} %slice.102), channel_id=1, source_target_pairs={{0,4},{4,8},{8,12},{12,16},{16,20},{20,24},{24,28},{1,5},{5,9},{9,... | collective-permute-start | bytes 23048 | tf_op jit(solution)/shard_map/ppermute | solution.py:22
  112.4 5.3 %copy-start.8 = (bf16[768,384]{1,0:T(8,128)(2,1)S(1)}, bf16[768,384]{1,0:T(8,128)(2,1)}, u32[]{:S(2)}) copy-start(bf16[768,384]{1,0:T(8,128)(2,1)} %param.29) | copy-start | bytes 1769476
  112.4 7.4 %copy-start.6 = (f32[96]{0:T(128)S(1)}, f32[96]{0:T(128)}, u32[]{:S(2)}) copy-start(f32[96]{0:T(128)} %param.32) | copy-start | bytes 1156
  120.9 85.9 %copy-start.5 = (f32[96]{0:T(128)S(1)}, f32[96]{0:T(128)}, u32[]{:S(2)}) copy-start(f32[96]{0:T(128)} %param.33) | copy-start | bytes 1156
  206.9 17.7 %copy-start.3 = (bf16[256,2048]{1,0:T(8,128)(2,1)S(1)}, bf16[256,2048]{1,0:T(8,128)(2,1)}, u32[]{:S(2)}) copy-start(bf16[256,2048]{1,0:T(8,128)(2,1)} %param.35) | copy-start | bytes 3145732
  208.2 2.4 copy-start.4
Sparse Core Ops, SparseCore 0:
  57.4 19.5 all-gather.7
  79.2 61.9 all-gather.3
  143.4 58.6 all-gather.5
  230.2 86.9 reduce-scatter.1
